TPU v7x, 512 devices: a whole 4x4x16 slice. The times are simulated.
512 devices in a mesh: dp: 4 (over x), kv: 64 (over z, y), tp: 2 (over core).
Axes of the slice: x: 4, y: 4, z: 16, core: 2. Of those that a mesh axis runs over, the one named last changes fastest.
Arguments:
- tokens: bfloat16 [16, 24, 2048], P('dp'), may hold values from -6 to 6
- norm_gain: bfloat16 [2048], replicated, may hold values from 0.099609375 to 1.8984375
- w_query: bfloat16 [2048, 1024], P('kv', 'tp'), may hold values from -0.125 to 0.125
- w_key: bfloat16 [2048, 1024], P('kv', 'tp'), may hold values from -0.03125 to 0.03125
- w_value: bfloat16 [2048, 1024], P('kv', 'tp'), may hold values from -0.03125 to 0.03125
- w_forget: bfloat16 [2048, 16], P('kv', 'tp'), may hold values from -0.125 to 0.125
- forget_bias: float32 [16], P('tp'), may hold values from 0 to 4
- head_gain: bfloat16 [1024], P('tp'), may hold values from 0.099609375 to 1.8984375
- w_out: bfloat16 [1024, 2048], P('tp', 'kv'), may hold values from -0.1875 to 0.1875
- cache_keys: bfloat16 [16, 16384, 1024], P('dp', 'kv', 'tp'), may hold values from -480 to 480
- cache_values: bfloat16 [16, 16384, 1024], P('dp', 'kv', 'tp'), may hold values from -1.5 to 1.5
- cache_gates: float32 [16, 16, 16384], P('dp', 'tp', 'kv'), may hold values from -2048 to 0, as said below
- lengths: int32 [16], P('dp'), may hold values from 8192 to 16335
- accepted: int32 [16], P('dp'), may hold values from 0 to 23
- parents: int32 [16, 24], P('dp'), may hold values from -1 to 22, as said below
Outputs:
- mixed: float32 [16, 24, 2048], P('dp', None, ('kv', 'tp'))
- keys_out: bfloat16 [16, 16384, 1024], P('dp', 'kv', 'tp')
- values_out: bfloat16 [16, 16384, 1024], P('dp', 'kv', 'tp')
- gates_out: float32 [16, 16, 16384], P('dp', 'tp', 'kv')
Inputs may be any that keep to these rules, and one draw needn't show every extreme that they name: parents[b, 0] = -1 and 0 <= parents[b, j] < j for every later proposal j. `cache_gates`: nonincreasing along the positions of each sequence and head.
All inputs are finite; a program needn't handle non-finite values.
Results may differ from a plain program's by a relative error of at most 0.008.
Values may be sent and summed in bfloat16 or wider, within the bound.
No kernel may reach another device: no remote copies, remote signals or barrier semaphores. Data moves between devices by JAX's collectives and lax.ppermute only.
A program may use at most 64 MiB of HBM per device.

v0:
```python
import jax
import jax.numpy as jnp
from jax import lax
from jax.sharding import Mesh
from jax.sharding import PartitionSpec as P

KV = ("kv_0", "kv_1")
KV_TP = ("kv_0", "kv_1", "tp")
NEG_LARGE = -1e30
EPSILON = 1e-06


def in_one_piece(arrays, axis, dim, along):
    widths = [a.shape[along] for a in arrays]
    both = jnp.concatenate(arrays, axis=along)
    whole = lax.all_gather(both, axis, axis=dim, tiled=True)
    return tuple(jnp.split(whole, [sum(widths[:k]) for k in range(1, len(widths))], axis=along))


def one_axis_at_a_time(array, axes):
    for axis in axes:
        array = lax.psum(array, axis)
    return array


def collected_together(array, axis):
    leaves = jax.tree.leaves(array)
    sequence = sorted(range(len(leaves)), key=lambda k: -leaves[k].size)
    width = (1, *leaves[sequence[0]].shape)[-1]
    lines = [
        jnp.pad(leaves[k].reshape(-1), (0, -leaves[k].size % width)).reshape(-1, width)
        for k in sequence
    ]
    both, at, found = (lax.all_gather(jnp.concatenate(lines), axis), 0, {})
    for k, line in zip(sequence, lines):
        piece = both[:, at : at + len(line)].reshape(len(both), -1)
        found[k] = piece[:, : leaves[k].size].reshape(-1, *leaves[k].shape)
        at += len(line)
    numbers = iter(range(len(leaves)))
    return jax.tree.map(lambda _: found[next(numbers)], array)


def merged_by_axis(array, axes, combine):
    for axis in axes:
        pieces = collected_together(array, axis)
        array = jax.tree.map(lambda part: part[0], pieces)
        for k in range(1, lax.axis_size(axis)):
            array = combine(array, jax.tree.map(lambda part: part[k], pieces))
    return array


def in_blocks(array, dim, peers):
    before, after = (array.shape[:dim], array.shape[dim + 1 :])
    return jnp.moveaxis(array.reshape(*before, peers, -1, *after), dim, 0)


def sent_and_summed(array, axis, dim):
    pieces = in_blocks(array, dim, lax.axis_size(axis))
    arrived = lax.all_to_all(pieces, axis, split_axis=0, concat_axis=0, tiled=True)
    return arrived.sum(axis=0)


def ancestry(parents):
    prop_count = parents.shape[1]
    indices = jnp.arange(prop_count, dtype=jnp.int32)
    linked = (parents[:, :, None] == indices[None, None, :]).astype(jnp.float32)
    linked = linked + (indices[:, None] == indices[None, :]).astype(jnp.float32)[None]
    for repeat in range(prop_count.bit_length()):
        linked = jnp.minimum(jnp.einsum("bij,bjk->bik", linked, linked), 1.0)
    return linked


def merge_pair(first_part, second_part):
    highest = jnp.maximum(first_part[0], second_part[0])
    scale_first = jnp.exp(first_part[0] - highest)
    scale_second = jnp.exp(second_part[0] - highest)
    seq_count, prop_count, head_count = highest.shape
    outer_first = (
        first_part[2].reshape(seq_count, prop_count, head_count, -1) * scale_first[..., None]
    )
    outer_second = (
        second_part[2].reshape(seq_count, prop_count, head_count, -1) * scale_second[..., None]
    )
    joined = (outer_first + outer_second).reshape(seq_count, prop_count, -1)
    return (highest, first_part[1] * scale_first + second_part[1] * scale_second, joined)


def local(
    tokens,
    norm_gain,
    w_query,
    w_key,
    w_value,
    w_forget,
    forget_bias,
    head_gain,
    w_out,
    cache_keys,
    cache_values,
    cache_gates,
    lengths,
    accepted,
    parents,
):
    seq_count, prop_count, model_width = tokens.shape
    span_rows = cache_keys.shape[1]
    head_count = cache_gates.shape[1]
    head_size = cache_keys.shape[2] // head_count
    scale = head_size ** (-0.5)
    start_pos = lax.axis_index(KV) * span_rows
    positions = start_pos + jnp.arange(span_rows, dtype=jnp.int32)
    valid_len = lengths + accepted
    flat_rows = tokens.reshape(seq_count * prop_count, model_width).astype(jnp.float32)
    normed = (
        flat_rows
        * lax.rsqrt(jnp.mean(flat_rows * flat_rows, axis=1, keepdims=True) + EPSILON)
        * norm_gain.astype(jnp.float32)
    ).astype(jnp.bfloat16)
    picked = (positions[None, :] == (valid_len - 1)[:, None]).astype(jnp.float32)
    last_part = jnp.sum(cache_gates * picked[:, None, :], axis=2)
    pieces = in_one_piece((w_query, w_key, w_value, w_forget), KV, 0, 1)
    query, fresh_keys, fresh_values, gate_pre = tuple(
        (jnp.dot(normed, piece, preferred_element_type=jnp.float32) for piece in pieces)
    )
    last_gate = one_axis_at_a_time(last_part, KV)
    query = query.astype(jnp.bfloat16).reshape(seq_count, prop_count, head_count, head_size)
    fresh_keys = fresh_keys.astype(jnp.bfloat16).reshape(
        seq_count, prop_count, head_count, head_size
    )
    fresh_values = fresh_values.astype(jnp.bfloat16).reshape(
        seq_count, prop_count, head_count, head_size
    )
    log_gate = jax.nn.log_sigmoid(gate_pre + forget_bias).reshape(seq_count, prop_count, head_count)
    link = ancestry(parents)
    climb = jnp.einsum("bia,bah->bih", link, log_gate)
    stored_keys = cache_keys.reshape(seq_count, span_rows, head_count, head_size)
    stored_values = cache_values.reshape(seq_count, span_rows, head_count, head_size)
    scores = (
        jnp.einsum("bphd,bchd->bphc", query, stored_keys, preferred_element_type=jnp.float32)
        * scale
    )
    scores = scores + (last_gate[:, None, :] + climb)[..., None] - cache_gates[:, None]
    seen = (positions[None, :] < valid_len[:, None])[:, None, None, :]
    highest = jnp.max(jnp.where(seen, scores, NEG_LARGE), axis=3)
    weights = jnp.where(seen, jnp.exp(scores - highest[..., None]), 0.0)
    normalizer = jnp.sum(weights, axis=3)
    weighted = jnp.einsum(
        "bphc,bchd->bphd",
        weights.astype(jnp.bfloat16),
        stored_values,
        preferred_element_type=jnp.float32,
    )
    highest, normalizer, weighted = merged_by_axis(
        (highest, normalizer, weighted.reshape(seq_count, prop_count, head_count * head_size)),
        KV,
        merge_pair,
    )
    near_scores = (
        jnp.einsum("bphd,bahd->bpha", query, fresh_keys, preferred_element_type=jnp.float32) * scale
    )
    near_scores = near_scores + climb[..., None] - jnp.transpose(climb, (0, 2, 1))[:, None]
    linked = (link > 0.5)[:, :, None, :]
    near_high = jnp.max(jnp.where(linked, near_scores, NEG_LARGE), axis=3)
    overall = jnp.maximum(highest, near_high)
    carried = jnp.exp(highest - overall)
    near_weights = jnp.where(linked, jnp.exp(near_scores - overall[..., None]), 0.0)
    normalizer = normalizer * carried + jnp.sum(near_weights, axis=3)
    attended = weighted.reshape(seq_count, prop_count, head_count, head_size) * carried[..., None]
    attended = attended + jnp.einsum(
        "bpha,bahd->bphd",
        near_weights.astype(jnp.bfloat16),
        fresh_values,
        preferred_element_type=jnp.float32,
    )
    attended = attended / normalizer[..., None]
    gain_rows = head_gain.astype(jnp.float32).reshape(head_count, head_size)
    heads_out = (
        (
            attended
            * lax.rsqrt(jnp.mean(attended * attended, axis=3, keepdims=True) + EPSILON)
            * gain_rows
        )
        .astype(jnp.bfloat16)
        .reshape(seq_count * prop_count, head_count * head_size)
    )
    partial_sum = jnp.dot(heads_out, w_out, preferred_element_type=jnp.float32)
    summed = sent_and_summed(partial_sum, "tp", 1)
    mixed = summed.reshape(seq_count, prop_count, -1)
    offsets = positions[None, :, None] - valid_len[:, None, None]
    placed = offsets == jnp.arange(prop_count, dtype=jnp.int32)[None, None, :]
    landed = jnp.any(placed, axis=2)
    placed_low = placed.astype(jnp.bfloat16)
    written_keys = jnp.einsum(
        "bcj,bjx->bcx",
        placed_low,
        fresh_keys.reshape(seq_count, prop_count, -1),
        preferred_element_type=jnp.float32,
    ).astype(jnp.bfloat16)
    written_values = jnp.einsum(
        "bcj,bjx->bcx",
        placed_low,
        fresh_values.reshape(seq_count, prop_count, -1),
        preferred_element_type=jnp.float32,
    ).astype(jnp.bfloat16)
    keys_out = jnp.where(landed[..., None], written_keys, cache_keys)
    values_out = jnp.where(landed[..., None], written_values, cache_values)
    new_gates = last_gate[:, :, None] + jnp.transpose(climb, (0, 2, 1))
    written_gates = jnp.einsum("bcj,bhj->bhc", placed.astype(jnp.float32), new_gates)
    gates_out = jnp.where(landed[:, None, :], written_gates, cache_gates)
    return (mixed, keys_out, values_out, gates_out)


def solution(mesh):
    torus = Mesh(
        mesh.devices.reshape(mesh.shape["dp"], 16, 4, mesh.shape["tp"]),
        ("dp", "kv_0", "kv_1", "tp"),
    )
    return jax.shard_map(
        local,
        mesh=torus,
        in_specs=(
            P("dp", None, None),
            P(),
            P(KV, "tp"),
            P(KV, "tp"),
            P(KV, "tp"),
            P(KV, "tp"),
            P("tp"),
            P("tp"),
            P("tp", KV),
            P("dp", KV, "tp"),
            P("dp", KV, "tp"),
            P("dp", "tp", KV),
            P("dp"),
            P("dp"),
            P("dp", None),
        ),
        out_specs=(P("dp", None, KV_TP), P("dp", KV, "tp"), P("dp", KV, "tp"), P("dp", "tp", KV)),
        check_vma=False,
    )
```

profile of v0, /device:TPU:1, one launch (start us, length us, event | category | flops | bytes accessed | tf_op | source)
XLA Modules:
  0.0 345.5 jit_solution(17081064558434147819)
XLA Ops:
  8.2 1.4 pad_maximum_fusion
  11.6 2.3 copy.57
  15.3 30.6 %psum.14 = f32[4,8]{1,0:T(4,128)S(1)} all-reduce(f32[4,8]{1,0:T(4,128)S(1)} %multiply_reduce_fusion.2), channel_id=1, replica_groups=mesh['dp'=4,'kv_0'=16,'kv_1'=4,'tp'=2] {'kv_0'}, use_global_device_ids=true, to_apply=%region_2.0 | all-reduce | flops 32 | bytes 256 | tf_op jit(solution)/shard_map/psum | solution.py:22
  45.8 9.1 %psum.15 = f32[4,8]{1,0:T(4,128)S(1)} all-reduce(f32[4,8]{1,0:T(4,128)S(1)} %psum.14), channel_id=1, replica_groups=mesh['dp'=4,'kv_0'=16,'kv_1'=4,'tp'=2] {'kv_1'}, use_global_device_ids=true, to_apply=%region_3.0 | all-reduce | flops 32 | bytes 256 | tf_op jit(solution)/shard_map/psum | solution.py:22
  56.5 104.4 %all-gather.7.cloned.1.call-done = bf16[2048,1544]{1,0:T(8,128)(2,1)} async-done(((bf16[32,1544]{1,0:T(8,128)(2,1)}), bf16[2048,1544]{1,0:T(8,128)(2,1)}) %all-gather.7.cloned.1.call-update) | async-done | bytes 6324240 | tf_op jit(solution)/shard_map/all_gather | solution.py:16
  162.3 2.1 fusion.16
  165.3 1.6 select_reduce_fusion
  167.6 1.6 fusion.28
  170.6 1.5 reshape.1556
  174.6 1.5 reshape.1554
  180.0 1.4 maximum_bitcast_fusion
  183.8 2.1 fusion.19
  186.1 2.1 fusion.22
  189.8 1.6 select_reduce_fusion.1
  191.4 1.5 fusion.6
  192.9 1.5 fusion.7
  194.4 57.1 %all-gather.9.cloned.1.call-done = f32[16,100,512]{2,1,0:T(8,128)} async-done(((f32[1,100,512]{2,1,0:T(8,128)}), f32[16,100,512]{2,1,0:T(8,128)}) %all-gather.9.cloned.1.call-update) | async-done | bytes 3276816 | tf_op jit(solution)/shard_map/all_gather | solution.py:34
  280.8 2.0 mul.671
  282.7 1.7 mul.664
  284.5 1.8 mul.665
  286.3 1.7 mul.667
  288.0 1.8 mul.668
  289.8 1.7 mul.658
  291.5 1.8 mul.659
  293.3 1.7 mul.652
  295.1 1.8 mul.653
  297.8 2.0 mul.656
  300.7 1.8 mul.647
  302.5 3.8 %fusion.45 = f32[96,512]{1,0:T(8,128)S(1)} fusion(f32[96,512]{1,0:T(8,128)} %mul.731, f32[16,100,512]{2,1,0:T(8,128)S(1)} %copy-done.3, f32[96,512]{1,0:T(8,128)} %mul.728, f32[96,512]{1,0:T(8,128)} %mul.725, f32[96,512]{1,0:T(8,128)} %mul.722, f32[96,512]{1,0:T(8,128)} %mul.719, f32[96,512]{1,0:T(8,128)} %mul.716, f32[96,512]{1,0:T(8,128)} %mul.713, ...), kind=kLoop, calls=%fused_computation.66 | loop fusion | flops 2211840 | bytes 9240576 | tf_op jit(solution)/shard_map/add | solution.py:84
  306.4 11.0 %all-gather.3 = f32[4,100,512]{2,1,0:T(8,128)S(1)} all-gather(f32[1,100,512]{2,1,0:T(8,128)S(1)} %maximum_bitcast_fusion.1), channel_id=3, replica_groups=mesh['dp'=4,'kv_0'=16,'kv_1'=4,'tp'=2] {'kv_1'}, dimensions={0}, use_global_device_ids=true | all-gather | bytes 1024000 | tf_op jit(solution)/shard_map/all_gather | solution.py:34
  319.6 1.7 multiply_reduce_fusion.1
  321.9 16.0 %all_to_all.5 = f32[2,96,16]{1,2,0:T(8,128)S(1)} all-to-all(f32[2,96,16]{1,2,0:T(8,128)S(1)} %convolution_bitcast_fusion.2), channel_id=1, replica_groups=mesh['dp'=4,'kv_0'=16,'kv_1'=4,'tp'=2] {'tp'}, dimensions={0} | all-to-all | bytes 24576 | tf_op jit(solution)/shard_map/all_to_all | solution.py:59
  (201 shorter events, 54.9 us)
Async XLA Ops:
  7.2 314.6 %copy-start = (bf16[512,32]{0,1:T(8,128)(2,1)S(1)}, bf16[512,32]{0,1:T(8,128)(2,1)}, u32[]{:S(2)}) copy-start(bf16[512,32]{0,1:T(8,128)(2,1)} %param.23) | copy-start | bytes 98308
  7.2 49.1 %copy-start.4 = (bf16[4,24,2048]{2,1,0:T(8,128)(2,1)S(1)}, bf16[4,24,2048]{2,1,0:T(8,128)(2,1)}, u32[]{:S(2)}) copy-start(bf16[4,24,2048]{2,1,0:T(8,128)(2,1)} %param.15) | copy-start | bytes 1179652
  7.2 6.7 %copy-start.2 = (bf16[4,256,512]{2,1,0:T(8,128)(2,1)S(1)}, bf16[4,256,512]{2,1,0:T(8,128)(2,1)}, u32[]{:S(2)}) copy-start(bf16[4,256,512]{2,1,0:T(8,128)(2,1)} %param.25) | copy-start | bytes 3145732
  7.2 7.2 %copy-start.18 = (s32[4]{0:T(128)S(1)}, s32[4]{0:T(128)}, u32[]{:S(2)}) copy-start(s32[4]{0:T(128)} %param.28) | copy-start | bytes 52
  7.2 7.2 %copy-start.17 = (s32[4]{0:T(128)S(1)}, s32[4]{0:T(128)}, u32[]{:S(2)}) copy-start(s32[4]{0:T(128)} %param.27) | copy-start | bytes 52
  7.2 7.9 %copy-start.6 = (f32[4,8,256]{2,1,0:T(8,128)S(1)}, f32[4,8,256]{2,1,0:T(8,128)}, u32[]{:S(2)}) copy-start(f32[4,8,256]{2,1,0:T(8,128)} %param.26) | copy-start | bytes 98308
  7.2 47.6 %copy-start.19 = (s32[4,24]{1,0:T(4,128)S(1)}, s32[4,24]{1,0:T(4,128)}, u32[]{:S(2)}) copy-start(s32[4,24]{1,0:T(4,128)} %param.29) | copy-start | bytes 1156
  7.2 153.6 %copy-start.16 = (f32[8]{0:T(128)S(1)}, f32[8]{0:T(128)}, u32[]{:S(2)}) copy-start(f32[8]{0:T(128)} %param.21) | copy-start | bytes 100
  7.3 153.6 %all-gather.7.cloned.1.call-start = ((), (), s32[]{:S(2)}) async-start(), calls=%async_computation.1 | async-start | bytes 6922240 | tf_op jit(solution)/shard_map/all_gather | solution.py:16
  9.6 241.9 %all-gather.9.cloned.1.call-start = ((), (), s32[]{:S(2)}) async-start(), calls=%async_computation.2 | async-start | bytes 3620864 | tf_op jit(solution)/shard_map/all_gather | solution.py:34
  14.5 147.8 %copy-start.15 = (s32[256]{0:T(256)}, s32[256]{0:T(256)S(1)}, u32[]{:S(2)}) copy-start(s32[256]{0:T(256)S(1)} %iota_add_fusion) | copy-start | bytes 3076
  14.5 0.7 copy-start.14
  54.9 110.4 %copy-start.9 = (f32[4,8]{1,0:T(4,128)}, f32[4,8]{1,0:T(4,128)S(1)}, u32[]{:S(2)}) copy-start(f32[4,8]{1,0:T(4,128)S(1)} %psum.15) | copy-start | bytes 388
  181.5 7.6 %copy-start.8 = (f32[4,24,8]{1,2,0:T(8,128)S(1)}, f32[4,24,8]{1,2,0:T(8,128)}, u32[]{:S(2)}) copy-start(f32[4,24,8]{1,2,0:T(8,128)} %get-tuple-element.142) | copy-start | bytes 9220
  181.5 7.6 %copy-start.10 = (f32[4,8]{1,0:T(4,128)S(1)}, f32[4,8]{1,0:T(4,128)}, u32[]{:S(2)}) copy-start(f32[4,8]{1,0:T(4,128)} %copy-done.9) | copy-start | bytes 388
  183.8 7.6 %copy-start.1 = (bf16[4,256,512]{2,1,0:T(8,128)(2,1)S(1)}, bf16[4,256,512]{2,1,0:T(8,128)(2,1)}, u32[]{:S(2)}) copy-start(bf16[4,256,512]{2,1,0:T(8,128)(2,1)} %param.24) | copy-start | bytes 3145732
  280.8 21.7 %copy-start.3 = (f32[16,100,512]{2,1,0:T(8,128)S(1)}, f32[16,100,512]{2,1,0:T(8,128)}, u32[]{:S(2)}) copy-start(f32[16,100,512]{2,1,0:T(8,128)} %all-gather.9.cloned.1.call-done) | copy-start | bytes 9830404
  302.5 3.8 %copy-start.11 = (f32[2,512]{1,0:T(2,128)S(1)}, f32[2,512]{1,0:T(2,128)}, u32[]{:S(2)}) copy-start(f32[2,512]{1,0:T(2,128)} %reshape.1561) | copy-start | bytes 12292
  302.5 3.8 %copy-start.12 = (f32[2,512]{1,0:T(2,128)S(1)}, f32[2,512]{1,0:T(2,128)}, u32[]{:S(2)}) copy-start(f32[2,512]{1,0:T(2,128)} %reshape.1559) | copy-start | bytes 12292
  306.3 13.1 %copy-start.13 = (f32[4,24,8]{1,2,0:T(8,128)S(1)}, f32[4,24,8]{1,2,0:T(8,128)}, u32[]{:S(2)}) copy-start(f32[4,24,8]{1,2,0:T(8,128)} %get-tuple-element.147) | copy-start | bytes 9220
  306.4 13.1 %copy-start.5 = (f32[4,24,8,24]{1,3,2,0:T(8,128)S(1)}, f32[4,24,8,24]{1,3,2,0:T(8,128)}, u32[]{:S(2)}) copy-start(f32[4,24,8,24]{1,3,2,0:T(8,128)} %get-tuple-element.148) | copy-start | bytes 221188
  306.4 13.2 %copy-start.7 = (bf16[4,24,8,64]{3,2,1,0:T(8,128)(2,1)S(1)}, bf16[4,24,8,64]{3,2,1,0:T(8,128)(2,1)}, u32[]{:S(2)}) copy-start(bf16[4,24,8,64]{3,2,1,0:T(8,128)(2,1)} %reshape.1564) | copy-start | bytes 294916
Sparse Core Ops, SparseCore 0:
  11.6 149.2 all-gather.6
  181.6 69.8 all-gather.8
where the time goes:
time: 347 us; the launch traced here: 345 us
  waiting for transfers between devices  162 us (47%)
  local copies, waits for them, and re-layouts  68.7 us (20%)
  blocking collectives  66.7 us (19%)
  matrix products  19.6 us (6%)
  between operations  14.9 us (4%)
  other arithmetic  13.9 us (4%)
    all_gather x1, waiting for transfers between devices, in_one_piece(): whole = lax.all_gather(both, axis, axis=dim, tiled=True)  104 us
    all_gather x1, waiting for transfers between devices, collected_together(): both, at, found = (lax.all_gather(jnp.concatenate(lines), axis), 0, {})  57.1 us
    psum x2, blocking collectives, one_axis_at_a_time(): array = lax.psum(array, axis)  39.6 us
    mul x30, local copies, waits for them, and re-layouts, merge_pair(): second_part[2].reshape(seq_count, prop_count, head_count, -1)  26 us
    mul x30, local copies, waits for them, and re-layouts, merge_pair(): first_part[2].reshape(seq_count, prop_count, head_count, -1)  19.1 us
    all_to_all x1, blocking collectives, sent_and_summed(): lax.all_to_all(pieces, axis, split_axis=0, concat_axis=0, tiled=True)  16 us
    all_gather x1, blocking collectives, collected_together(): both, at, found = (lax.all_gather(jnp.concatenate(lines), axis), 0, {})  11 us
    dot_general x4, matrix products, local(): jnp.dot(normed, piece, preferred_element_type=jnp.float32)  7.6 us
  transfers between devices with their start and end apart: 2, of which 2 were waited for; matrix products, arithmetic and copies ran while one was open for 6% of the time, Pallas kernels for 0%

commit v1 on v0

--- a/solution.py
+++ b/solution.py
@@ -19,7 +19,7 @@
 
 def one_axis_at_a_time(array, axes):
     for axis in axes:
-        array = lax.psum(array, axis)
+        array = jnp.sum(lax.all_gather(array, axis), axis=0)
     return array
 
 

time: 347 us -> 347 us (level)
    psum x2 -> x0, blocking collectives: 39.6 us -> none  [one_axis_at_a_time(): array = lax.psum(array, axis)]
    all_gather x0 -> x2, blocking collectives: none -> 39.4 us  [one_axis_at_a_time(): array = jnp.sum(lax.all_gather(array, axis), axis=0)]
where the time goes in v1:
time: 347 us; the launch traced here: 345 us
  waiting for transfers between devices  160 us (46%)
  local copies, waits for them, and re-layouts  68.7 us (20%)
  blocking collectives  66.4 us (19%)
  matrix products  19.6 us (6%)
  other arithmetic  15.4 us (4%)
  between operations  14.9 us (4%)
    all_gather x1, waiting for transfers between devices, in_one_piece(): whole = lax.all_gather(both, axis, axis=dim, tiled=True)  103 us
    all_gather x1, waiting for transfers between devices, collected_together(): both, at, found = (lax.all_gather(jnp.concatenate(lines), axis), 0, {})  57.1 us
    all_gather x2, blocking collectives, one_axis_at_a_time(): array = jnp.sum(lax.all_gather(array, axis), axis=0)  39.4 us
    mul x30, local copies, waits for them, and re-layouts, merge_pair(): second_part[2].reshape(seq_count, prop_count, head_count, -1)  26 us
    mul x30, local copies, waits for them, and re-layouts, merge_pair(): first_part[2].reshape(seq_count, prop_count, head_count, -1)  19.1 us
    all_to_all x1, blocking collectives, sent_and_summed(): lax.all_to_all(pieces, axis, split_axis=0, concat_axis=0, tiled=True)  16 us
    all_gather x1, blocking collectives, collected_together(): both, at, found = (lax.all_gather(jnp.concatenate(lines), axis), 0, {})  11 us
    dot_general x4, matrix products, local(): jnp.dot(normed, piece, preferred_element_type=jnp.float32)  7.59 us
  transfers between devices with their start and end apart: 2, of which 2 were waited for; matrix products, arithmetic and copies ran while one was open for 6% of the time, Pallas kernels for 0%

profile of v1, /device:TPU:1, one launch (start us, length us, event | category | flops | bytes accessed | tf_op | source)
XLA Modules:
  0.0 345.5 jit_solution(4843076343569136830)
XLA Ops:
  8.1 1.4 pad_maximum_fusion
  13.8 29.4 %all-gather.4 = f32[16,4,8]{2,1,0:T(4,128)S(1)} all-gather(f32[1,4,8]{2,1,0:T(4,128)S(1)} %bitcast.303), channel_id=2, replica_groups=mesh['dp'=4,'kv_0'=16,'kv_1'=4,'tp'=2] {'kv_0'}, dimensions={0}, use_global_device_ids=true | all-gather | bytes 2176 | tf_op jit(solution)/shard_map/all_gather | solution.py:22
  43.3 9.9 %all-gather.5 = f32[4,4,8]{2,1,0:T(4,128)S(1)} all-gather(f32[1,4,8]{2,1,0:T(4,128)S(1)} %bitcast.304), channel_id=3, replica_groups=mesh['dp'=4,'kv_0'=16,'kv_1'=4,'tp'=2] {'kv_1'}, dimensions={0}, use_global_device_ids=true | all-gather | bytes 640 | tf_op jit(solution)/shard_map/all_gather | solution.py:22
  53.2 2.3 copy.57
  57.6 103.2 %all-gather.11.cloned.1.call-done = bf16[2048,1544]{1,0:T(8,128)(2,1)} async-done(((bf16[32,1544]{1,0:T(8,128)(2,1)}), bf16[2048,1544]{1,0:T(8,128)(2,1)}) %all-gather.11.cloned.1.call-update) | async-done | bytes 6324240 | tf_op jit(solution)/shard_map/all_gather | solution.py:16
  162.3 2.1 fusion.16
  165.2 1.6 select_reduce_fusion
  167.6 1.6 fusion.28
  170.6 1.5 reshape.1556
  174.6 1.5 reshape.1554
  180.0 1.4 maximum_bitcast_fusion
  183.8 2.1 fusion.19
  186.1 2.1 fusion.22
  189.8 1.6 select_reduce_fusion.1
  191.4 1.5 fusion.6
  192.9 1.5 fusion.7
  194.4 57.1 %all-gather.13.cloned.1.call-done = f32[16,100,512]{2,1,0:T(8,128)} async-done(((f32[1,100,512]{2,1,0:T(8,128)}), f32[16,100,512]{2,1,0:T(8,128)}) %all-gather.13.cloned.1.call-update) | async-done | bytes 3276816 | tf_op jit(solution)/shard_map/all_gather | solution.py:34
  280.8 2.0 mul.671
  282.7 1.7 mul.664
  284.5 1.8 mul.665
  286.3 1.7 mul.667
  288.0 1.8 mul.668
  289.8 1.7 mul.658
  291.5 1.8 mul.659
  293.3 1.7 mul.652
  295.0 1.8 mul.653
  297.8 2.0 mul.656
  300.7 1.8 mul.647
  302.5 3.8 %fusion.45 = f32[96,512]{1,0:T(8,128)S(1)} fusion(f32[96,512]{1,0:T(8,128)} %mul.731, f32[16,100,512]{2,1,0:T(8,128)S(1)} %copy-done.3, f32[96,512]{1,0:T(8,128)} %mul.728, f32[96,512]{1,0:T(8,128)} %mul.725, f32[96,512]{1,0:T(8,128)} %mul.722, f32[96,512]{1,0:T(8,128)} %mul.719, f32[96,512]{1,0:T(8,128)} %mul.716, f32[96,512]{1,0:T(8,128)} %mul.713, ...), kind=kLoop, calls=%fused_computation.66 | loop fusion | flops 2211840 | bytes 9240576 | tf_op jit(solution)/shard_map/add | solution.py:84
  306.4 11.0 %all-gather.7 = f32[4,100,512]{2,1,0:T(8,128)S(1)} all-gather(f32[1,100,512]{2,1,0:T(8,128)S(1)} %maximum_bitcast_fusion.1), channel_id=5, replica_groups=mesh['dp'=4,'kv_0'=16,'kv_1'=4,'tp'=2] {'kv_1'}, dimensions={0}, use_global_device_ids=true | all-gather | bytes 1024000 | tf_op jit(solution)/shard_map/all_gather | solution.py:34
  319.6 1.7 multiply_reduce_fusion.1
  321.9 16.0 %all_to_all.5 = f32[2,96,16]{1,2,0:T(8,128)S(1)} all-to-all(f32[2,96,16]{1,2,0:T(8,128)S(1)} %convolution_bitcast_fusion.2), channel_id=1, replica_groups=mesh['dp'=4,'kv_0'=16,'kv_1'=4,'tp'=2] {'tp'}, dimensions={0} | all-to-all | bytes 24576 | tf_op jit(solution)/shard_map/all_to_all | solution.py:59
  (199 shorter events, 56.3 us)
Async XLA Ops:
  7.2 314.6 %copy-start = (bf16[512,32]{0,1:T(8,128)(2,1)S(1)}, bf16[512,32]{0,1:T(8,128)(2,1)}, u32[]{:S(2)}) copy-start(bf16[512,32]{0,1:T(8,128)(2,1)} %param.23) | copy-start | bytes 98308
  7.2 50.2 %copy-start.4 = (bf16[4,24,2048]{2,1,0:T(8,128)(2,1)S(1)}, bf16[4,24,2048]{2,1,0:T(8,128)(2,1)}, u32[]{:S(2)}) copy-start(bf16[4,24,2048]{2,1,0:T(8,128)(2,1)} %param.15) | copy-start | bytes 1179652
  7.2 48.3 %copy-start.2 = (bf16[4,256,512]{2,1,0:T(8,128)(2,1)S(1)}, bf16[4,256,512]{2,1,0:T(8,128)(2,1)}, u32[]{:S(2)}) copy-start(bf16[4,256,512]{2,1,0:T(8,128)(2,1)} %param.25) | copy-start | bytes 3145732
  7.2 48.8 %copy-start.17 = (s32[4,24]{1,0:T(4,128)S(1)}, s32[4,24]{1,0:T(4,128)}, u32[]{:S(2)}) copy-start(s32[4,24]{1,0:T(4,128)} %param.29) | copy-start | bytes 1156
  7.2 153.6 %copy-start.16 = (f32[8]{0:T(128)S(1)}, f32[8]{0:T(128)}, u32[]{:S(2)}) copy-start(f32[8]{0:T(128)} %param.21) | copy-start | bytes 100
  7.2 153.6 %all-gather.11.cloned.1.call-start = ((), (), s32[]{:S(2)}) async-start(), calls=%async_computation.1 | async-start | bytes 6922240 | tf_op jit(solution)/shard_map/all_gather | solution.py:16
  9.6 241.9 %all-gather.13.cloned.1.call-start = ((), (), s32[]{:S(2)}) async-start(), calls=%async_computation.2 | async-start | bytes 3620864 | tf_op jit(solution)/shard_map/all_gather | solution.py:34
  11.6 2.2 copy-start.15
  12.3 0.7 copy-start.14
  53.2 111.3 %copy-start.9 = (f32[4,8]{1,0:T(4,128)}, f32[4,8]{1,0:T(4,128)S(1)}, u32[]{:S(2)}) copy-start(f32[4,8]{1,0:T(4,128)S(1)} %reduce_sum.75) | copy-start | bytes 388
  55.5 109.8 %copy-start.6 = (f32[4,8,256]{2,1,0:T(8,128)S(1)}, f32[4,8,256]{2,1,0:T(8,128)}, u32[]{:S(2)}) copy-start(f32[4,8,256]{2,1,0:T(8,128)} %param.26) | copy-start | bytes 98308
  181.4 7.6 %copy-start.8 = (f32[4,24,8]{1,2,0:T(8,128)S(1)}, f32[4,24,8]{1,2,0:T(8,128)}, u32[]{:S(2)}) copy-start(f32[4,24,8]{1,2,0:T(8,128)} %get-tuple-element.142) | copy-start | bytes 9220
  181.4 7.6 %copy-start.10 = (f32[4,8]{1,0:T(4,128)S(1)}, f32[4,8]{1,0:T(4,128)}, u32[]{:S(2)}) copy-start(f32[4,8]{1,0:T(4,128)} %copy-done.9) | copy-start | bytes 388
  183.8 7.6 %copy-start.1 = (bf16[4,256,512]{2,1,0:T(8,128)(2,1)S(1)}, bf16[4,256,512]{2,1,0:T(8,128)(2,1)}, u32[]{:S(2)}) copy-start(bf16[4,256,512]{2,1,0:T(8,128)(2,1)} %param.24) | copy-start | bytes 3145732
  280.8 21.7 %copy-start.3 = (f32[16,100,512]{2,1,0:T(8,128)S(1)}, f32[16,100,512]{2,1,0:T(8,128)}, u32[]{:S(2)}) copy-start(f32[16,100,512]{2,1,0:T(8,128)} %all-gather.13.cloned.1.call-done) | copy-start | bytes 9830404
  302.5 3.8 %copy-start.11 = (f32[2,512]{1,0:T(2,128)S(1)}, f32[2,512]{1,0:T(2,128)}, u32[]{:S(2)}) copy-start(f32[2,512]{1,0:T(2,128)} %reshape.1561) | copy-start | bytes 12292
  302.5 3.8 %copy-start.12 = (f32[2,512]{1,0:T(2,128)S(1)}, f32[2,512]{1,0:T(2,128)}, u32[]{:S(2)}) copy-start(f32[2,512]{1,0:T(2,128)} %reshape.1559) | copy-start | bytes 12292
  306.3 13.1 %copy-start.13 = (f32[4,24,8]{1,2,0:T(8,128)S(1)}, f32[4,24,8]{1,2,0:T(8,128)}, u32[]{:S(2)}) copy-start(f32[4,24,8]{1,2,0:T(8,128)} %get-tuple-element.147) | copy-start | bytes 9220
  306.4 13.1 %copy-start.5 = (f32[4,24,8,24]{1,3,2,0:T(8,128)S(1)}, f32[4,24,8,24]{1,3,2,0:T(8,128)}, u32[]{:S(2)}) copy-start(f32[4,24,8,24]{1,3,2,0:T(8,128)} %get-tuple-element.148) | copy-start | bytes 221188
  306.4 13.2 %copy-start.7 = (bf16[4,24,8,64]{3,2,1,0:T(8,128)(2,1)S(1)}, bf16[4,24,8,64]{3,2,1,0:T(8,128)(2,1)}, u32[]{:S(2)}) copy-start(bf16[4,24,8,64]{3,2,1,0:T(8,128)(2,1)} %reshape.1564) | copy-start | bytes 294916
Sparse Core Ops, SparseCore 0:
  11.6 149.2 all-gather.10
  181.6 69.8 all-gather.12
